TPU v7x, 256 devices: a whole 4x4x8 slice. The times are simulated.
256 devices in a mesh: sp: 64 (over z, x, core), tp: 4 (over y).
Axes of the slice: x: 4, y: 4, z: 8, core: 2. Of those that a mesh axis runs over, the one named last changes fastest.
Arguments:
- queries: bfloat16 [65536, 2048], P('sp', 'tp'), may hold values from -16 to 16
- key_rows: bfloat16 [65536, 512], P('sp', 'tp'), may hold values from -16 to 16
- value_rows: bfloat16 [65536, 512], P('sp', 'tp'), may hold values from -6 to 6
- doc_ids: int32 [65536], P('sp'), may hold values from 0 to 31, never falling along the last dimension, each value on 1 to 4096 neighbouring positions
- sink_logit: float32 [32], P('tp'), may hold values from 3 to 7
- residual: bfloat16 [65536, 2048], P(('sp', 'tp')), may hold values from -6 to 6
- out_weight: bfloat16 [2048, 2048], P('tp'), may hold values from -3.5 to 3.5
- norm_gain: float32 [2048], replicated, may hold values from 0.1 to 1.9
- gate_weight: bfloat16 [64, 2048, 512], P('sp'), may hold values from -0.125 to 0.125
- up_weight: bfloat16 [64, 2048, 512], P('sp'), may hold values from -0.125 to 0.125
- down_weight: bfloat16 [64, 512, 2048], P('sp'), may hold values from -0.25 to 0.25
- routes: int32 [65536, 2], P(('sp', 'tp')), may hold values from 0 to 63, as said below
- route_weights: float32 [65536, 2], P(('sp', 'tp')), may hold values from 0.2 to 0.8
Outputs:
- mixed: bfloat16 [65536, 2048], P(('sp', 'tp'))
Inputs may be any that keep to these rules, and one draw needn't show every extreme that they name: `doc_ids`: never falls along the positions. `routes`: each aligned block of 256 rows names every expert exactly 8 times; the experts of one row differ and lie in one group of 16 consecutive numbers.
All inputs are finite; a program needn't handle non-finite values.
Results may differ from a plain program's by a relative error of at most 0.012.
Values may be sent and summed in bfloat16 or wider, within the bound.
No kernel may reach another device: no remote copies, remote signals or barrier semaphores. Data moves between devices by JAX's collectives and lax.ppermute only.
A program may use at most 128 MiB of HBM per device.

v0:
```python
import jax
import jax.numpy as jnp
from jax import lax
from jax.sharding import PartitionSpec as P

HD = 64
WINDOW = 128


neg_fill = -1e30
eps_norm = 1e-06


def extended(block, sides, width):
    for axis, dim in sides:
        count = lax.axis_size(axis)
        forward = [(i, i + 1) for i in range(count - 1)]
        backward = [(target, source) for source, target in forward]
        low = lax.ppermute(
            lax.slice_in_dim(block, block.shape[dim] - width, None, axis=dim), axis, forward
        )
        high = lax.ppermute(lax.slice_in_dim(block, 0, width, axis=dim), axis, backward)
        block = jnp.concatenate([low, block, high], axis=dim)
    return block


def attend(
    query_part,
    key_part,
    value_part,
    query_docs,
    key_docs,
    query_start,
    key_start,
    sink_logit,
    extent,
):
    query_count = query_part.shape[0]
    key_count = key_part.shape[0]
    groups = key_part.shape[1] // HD
    head_ratio = sink_logit.shape[0] // groups
    query_heads = query_part.reshape(query_count, groups, head_ratio, HD)
    key_heads = key_part.reshape(key_count, groups, HD)
    value_heads = value_part.reshape(key_count, groups, HD)
    scores = jnp.einsum(
        "qgrd,kgd->grqk", query_heads, key_heads, preferred_element_type=jnp.float32
    ) * HD ** (-0.5)
    query_pos = query_start + jnp.arange(query_count, dtype=jnp.int32)
    key_pos = key_start + jnp.arange(key_count, dtype=jnp.int32)
    inside = (key_pos >= 0) & (key_pos < extent)
    allowed = (
        (jnp.abs(query_pos[:, None] - key_pos[None, :]) <= WINDOW)
        & (query_docs[:, None] == key_docs[None, :])
        & inside[None, :]
    )
    masked = jnp.where(allowed[None, None], scores, neg_fill)
    sink_col = sink_logit.reshape(groups, head_ratio)[:, :, None, None]
    row_top = jnp.maximum(jnp.max(masked, axis=3, keepdims=True), sink_col)
    exponent = jnp.where(allowed[None, None], jnp.exp(masked - row_top), 0.0)
    denominator = jnp.sum(exponent, axis=3, keepdims=True) + jnp.exp(sink_col - row_top)
    attn_weight = (exponent / denominator).astype(jnp.bfloat16)
    attended = jnp.einsum(
        "grqk,kgd->qgrd", attn_weight, value_heads, preferred_element_type=jnp.float32
    )
    return attended.astype(jnp.bfloat16).reshape(query_count, -1)


def fetch_margins(key_rows, value_rows, doc_float):
    return (
        extended(key_rows, (("sp", 0),), WINDOW),
        extended(value_rows, (("sp", 0),), WINDOW),
        extended(doc_float, (("sp", 0),), WINDOW),
    )


def per_device(
    queries,
    key_rows,
    value_rows,
    doc_ids,
    sink_logit,
    residual,
    out_weight,
    norm_gain,
    gate_weight,
    up_weight,
    down_weight,
    routes,
    route_weights,
):
    local_rows = queries.shape[0]
    anchor = lax.axis_index("sp") * local_rows
    extent = local_rows * lax.axis_size("sp")
    doc_float = doc_ids.astype(jnp.bfloat16)
    block_rows = min(512, local_rows)
    padded_keys, padded_values, padded_docs = fetch_margins(key_rows, value_rows, doc_float)
    block_parts = []
    for row_start in range(0, local_rows, block_rows):
        key_end = row_start + block_rows + 2 * WINDOW
        block_parts.append(
            attend(
                queries[row_start : row_start + block_rows],
                padded_keys[row_start:key_end],
                padded_values[row_start:key_end],
                doc_float[row_start : row_start + block_rows],
                padded_docs[row_start:key_end],
                anchor + row_start,
                anchor + row_start - WINDOW,
                sink_logit,
                extent,
            )
        )
    attended = jnp.concatenate(block_parts, axis=0)
    regrouped = lax.all_to_all(attended, "tp", split_axis=0, concat_axis=1, tiled=True)
    shard_rows = out_weight.shape[0]
    initial = jnp.zeros((regrouped.shape[0], out_weight.shape[1]), jnp.float32)
    running = initial
    weight_piece = lax.all_gather(out_weight, "tp", axis=0, tiled=True)
    for shard_index in range(weight_piece.shape[0] // shard_rows):
        columns = lax.dynamic_slice_in_dim(regrouped, shard_index * shard_rows, shard_rows, 1)
        partial_value = jnp.dot(
            columns,
            weight_piece[shard_index * shard_rows : (shard_index + 1) * shard_rows],
            preferred_element_type=jnp.float32,
        )
        running = running + partial_value.astype(jnp.bfloat16).astype(jnp.float32)
    stream = (residual.astype(jnp.float32) + running).astype(jnp.bfloat16)
    stream_f = stream.astype(jnp.float32)
    scale = lax.rsqrt(jnp.mean(stream_f * stream_f, axis=1, keepdims=True) + eps_norm)
    normed = (stream_f * scale * norm_gain[None, :]).astype(jnp.bfloat16)
    home_rows = normed.shape[0]
    width = normed.shape[1]
    route_count = routes.shape[1]
    expert_count = lax.axis_size("sp") * gate_weight.shape[0]
    capacity = route_count * home_rows // expert_count
    flat_routes = routes.reshape(-1)
    one_hot = (flat_routes[:, None] == jnp.arange(expert_count, dtype=jnp.int32)[None, :]).astype(
        jnp.int32
    )
    earlier = jnp.cumsum(one_hot, axis=0) - one_hot
    slot_rank = jnp.sum(earlier * one_hot, axis=1)
    slot_index = flat_routes * capacity + slot_rank
    source_row = (
        jnp.zeros((expert_count * capacity,), jnp.int32)
        .at[slot_index]
        .set(jnp.arange(home_rows * route_count, dtype=jnp.int32) // route_count)
    )
    outgoing = normed[source_row].reshape(expert_count, capacity, width)
    incoming = lax.all_to_all(outgoing, "sp", split_axis=0, concat_axis=0, tiled=True)
    flat_rows = incoming.reshape(-1, width)
    gate_act = jnp.dot(flat_rows, gate_weight[0], preferred_element_type=jnp.float32)
    up_act = jnp.dot(flat_rows, up_weight[0], preferred_element_type=jnp.float32)
    hidden = (jax.nn.silu(gate_act) * up_act).astype(jnp.bfloat16)
    produced = jnp.dot(hidden, down_weight[0], preferred_element_type=jnp.float32).astype(
        jnp.bfloat16
    )
    returned = lax.all_to_all(
        produced.reshape(incoming.shape), "sp", split_axis=0, concat_axis=0, tiled=True
    )
    route_out = returned.reshape(-1, width)[slot_index].reshape(home_rows, route_count, width)
    weighted = jnp.sum(route_weights[:, :, None] * route_out.astype(jnp.float32), axis=1)
    return (stream_f + weighted).astype(jnp.bfloat16)


def solution(mesh):
    return jax.shard_map(
        per_device,
        mesh=mesh,
        in_specs=(
            P("sp", "tp"),
            P("sp", "tp"),
            P("sp", "tp"),
            P("sp"),
            P("tp"),
            P(("sp", "tp"), None),
            P("tp", None),
            P(),
            P("sp", None, None),
            P("sp", None, None),
            P("sp", None, None),
            P(("sp", "tp"), None),
            P(("sp", "tp"), None),
        ),
        out_specs=P(("sp", "tp"), None),
        check_vma=False,
    )
```

profile of v0, /device:TPU:8, one launch (start us, length us, event | category | flops | bytes accessed | tf_op | source)
XLA Modules:
  0.0 281.0 jit_solution(16703556512398380717)
XLA Ops:
  6.5 0.7 all-gather.2.cloned.1.call-update
  7.4 0.6 fusion.75
  7.9 1.7 collective-permute-start.1
  9.7 1.3 collective-permute-start.4
  11.0 1.4 fusion.73
  12.4 4.3 %collective-permute-start.2 = (bf16[128,128]{1,0:T(8,128)(2,1)}, bf16[128,128]{1,0:T(8,128)(2,1)S(1)}, u32[]{:S(2)}, u32[]{:S(2)}) collective-permute-start(bf16[128,128]{1,0:T(8,128)(2,1)} %get-tuple-element.9), channel_id=1, source_target_pairs={{0,4},{4,8},{8,12},{12,16},{16,20},{20,24},{24,28},{28,32},{32,36}... | collective-permute-start | bytes 98312 | tf_op jit(solution)/shard_map/ppermute | solution.py:19
  16.7 1.3 collective-permute-start.5
  18.0 1.4 fusion.74
  19.4 4.3 %collective-permute-start = (bf16[128,128]{1,0:T(8,128)(2,1)}, bf16[128,128]{1,0:T(8,128)(2,1)S(1)}, u32[]{:S(2)}, u32[]{:S(2)}) collective-permute-start(bf16[128,128]{1,0:T(8,128)(2,1)} %get-tuple-element.13), channel_id=1, source_target_pairs={{0,4},{4,8},{8,12},{12,16},{16,20},{20,24},{24,28},{28,32},{32,36}... | collective-permute-start | bytes 98312 | tf_op jit(solution)/shard_map/ppermute | solution.py:19
  24.0 0.7 eq.65
  24.7 1.4 fusion.72
  26.1 1.0 copy.38
  27.2 0.7 max.32
  27.8 1.2 reduce-window.6
  29.0 0.6 compare_and_fusion
  29.7 0.6 compare_and_fusion.1
  30.2 0.6 iota_add_fusion.3
  30.8 0.6 iota_add_fusion.2
  31.4 0.2 slice_reduce_fusion
  31.6 0.6 fusion.76
  32.2 1.0 copy.42
  33.4 0.7 mul.81
  34.1 0.5 copy-done.23
  34.6 1.3 collective-permute-start.3
  35.9 0.7 pad_maximum_fusion.6
  36.6 2.3 fusion.33
  39.0 1.8 pad_maximum_fusion.3
  40.8 1.8 copy.37
  42.5 1.8 copy.41
  44.3 1.8 pad_maximum_fusion.4
  46.0 1.7 copy.36
  47.8 3.1 %fusion = (f32[2,4,512]{2,1,0:T(4,128)S(1)}, f32[2,768,512,4]{2,1,3,0:T(8,128)S(1)}) fusion(pred[512,768]{0,1:T(8,128)(4,1)S(1)} %get-tuple-element.30, bf16[768,2,64,1]{0,2,3,1:T(8,128)(2,1)} %bitcast.124, bf16[512,2,4,64]{0,3,2,1:T(8,128)(2,1)S(1)} %bitcast.121), kind=kOutput, calls=%fused_computation.9 | convolution fusion | flops 412086272 | bytes 13713408 | tf_op jit(solution)/shard_map/qgrd,kgd->grqk/dot_general | solution.py:45
  51.0 6.6 %fusion.1 = (f32[2,4,512]{2,1,0:T(4,128)S(1)}, f32[2,768,512,4]{2,1,3,0:T(8,128)}) fusion(pred[512,768]{0,1:T(8,128)(4,1)S(1)} %get-tuple-element.29, bf16[768,2,64,1]{0,2,3,1:T(8,128)(2,1)S(1)} %bitcast.123, bf16[512,2,4,64]{0,3,2,1:T(8,128)(2,1)S(1)} %bitcast.122), kind=kOutput, calls=%fused_computation.10 | convolution fusion | flops 412086272 | bytes 13713408 | tf_op jit(solution)/shard_map/qgrd,kgd->grqk/dot_general | solution.py:45
  57.6 3.1 %fusion.2 = f32[2,4,512]{2,1,0:T(4,128)S(1)} fusion(f32[2,768,512,4]{2,1,3,0:T(8,128)S(1)} %get-tuple-element.24, f32[2,4,512]{2,1,0:T(4,128)S(1)} %broadcast_maximum_fusion.1, pred[512,768]{0,1:T(8,128)(4,1)S(1)} %get-tuple-element.30), kind=kLoop, calls=%fused_computation.11 | loop fusion | flops 15724544 | bytes 13008896 | tf_op jit(solution)/shard_map/reduce_sum | solution.py:60
  60.8 4.7 %fusion.46 = bf16[2,64,4,512]{3,1,2,0:T(8,128)(2,1)} fusion(bf16[768,2,64,1]{0,2,3,1:T(8,128)(2,1)S(1)} %bitcast.127, f32[2,768,512,4]{2,1,3,0:T(8,128)S(1)} %get-tuple-element.24, f32[2,4,512]{2,1,0:T(4,128)S(1)} %get-tuple-element.21, f32[2,4,512]{2,1,0:T(4,128)S(1)} %broadcast_maximum_fusion.1, pred[512,768]{0,1:T(8,128)(4,1)S(1)} %get-tuple-element.30), kind=kOutput, calls=%fused_computation.58 | convolution fusion | flops 421789696 | bytes 13729792 | tf_op jit(solution)/shard_map/grqk,kgd->qgrd/dot_general | solution.py:62
  65.5 1.3 copy.44
  66.9 6.9 %fusion.3 = f32[2,4,512]{2,1,0:T(4,128)S(1)} fusion(f32[2,768,512,4]{2,1,3,0:T(8,128)} %get-tuple-element.26, f32[2,4,512]{2,1,0:T(4,128)S(1)} %get-tuple-element.22, pred[512,768]{0,1:T(8,128)(4,1)S(1)} %get-tuple-element.29), kind=kLoop, calls=%fused_computation.12 | loop fusion | flops 15724544 | bytes 13008896 | tf_op jit(solution)/shard_map/reduce_sum | solution.py:60
  73.9 1.4 copy-done.1
  75.3 4.6 %fusion.45 = bf16[2,64,4,512]{3,1,2,0:T(8,128)(2,1)} fusion(bf16[768,2,64,1]{0,2,3,1:T(8,128)(2,1)S(1)} %bitcast.128, f32[2,768,512,4]{2,1,3,0:T(8,128)S(1)} %copy-done.1, f32[2,4,512]{2,1,0:T(4,128)S(1)} %exponential_add_fusion, f32[2,4,512]{2,1,0:T(4,128)S(1)} %get-tuple-element.22, pred[512,768]{0,1:T(8,128)(4,1)S(1)} %get-tuple-element.29), kind=kOutput, calls=%fused_computation.57 | convolution fusion | flops 421789696 | bytes 13729792 | tf_op jit(solution)/shard_map/grqk,kgd->qgrd/dot_general | solution.py:62
  79.9 1.3 copy.45
  81.2 1.0 pad_maximum_fusion
  82.3 5.0 %all-to-all-start = ((bf16[4,256,512]{2,1,0:T(8,128)(2,1)}), bf16[4,256,512]{2,1,0:T(8,128)(2,1)S(1)}, u32[]{:S(2)}, u32[]{:S(2)}) async-start(bf16[4,256,512]{2,1,0:T(8,128)(2,1)} %bitcast.120), calls=%async_computation | async-start | bytes 2097152 | tf_op jit(solution)/shard_map/all_to_all | solution.py:114
  87.5 2.4 scatter_custom_fusion
  89.9 18.9 %all-to-all-done = bf16[4,256,512]{2,1,0:T(8,128)(2,1)S(1)} async-done(((bf16[4,256,512]{2,1,0:T(8,128)(2,1)}), bf16[4,256,512]{2,1,0:T(8,128)(2,1)S(1)}, u32[]{:S(2)}, u32[]{:S(2)}) %all-to-all-start) | async-done | bytes 1048608 | tf_op jit(solution)/shard_map/all_to_all | solution.py:114
  108.9 1.0 copy-done.5
  109.8 1.5 copy.46
  111.3 2.5 fusion.13
  113.8 2.9 %fusion.14 = f32[256,2048]{1,0:T(8,128)S(1)} fusion(bf16[2048,2048]{1,0:T(8,128)(2,1)} %all-gather.2.cloned.1.call-done, bf16[256,2048]{0,1:T(8,128)(2,1)S(1)} %bitcast.116), kind=kOutput, calls=%fused_computation.32 | convolution fusion | flops 537919488 | bytes 4456448 | tf_op jit(solution)/shard_map/dot_general | solution.py:121
  116.7 0.7 fusion.15
  117.4 0.5 copy-done.11
  117.9 1.2 fusion.16
  119.1 1.0 copy-done.2
  120.1 0.3 fusion.18
  120.4 3.3 %gather_fusion = bf16[512,2048]{1,0:T(8,128)(2,1)} fusion(bf16[256,2048]{1,0:T(8,128)(2,1)S(1)} %fusion.18, s32[1024]{0:T(1024)S(1)} %pad_clamp_fusion.1), kind=kCustom, calls=%fused_computation | custom fusion | bytes 4196352 | tf_op jit(solution)/shard_map/gather | solution.py:148
  123.7 62.2 %all_to_all.29 = bf16[64,8,2048]{2,1,0:T(8,128)(2,1)S(1)} all-to-all(bf16[64,8,2048]{2,1,0:T(8,128)(2,1)} %bitcast.114), channel_id=1, replica_groups=mesh['sp'=64,'tp'=4] {'sp'}, dimensions={0} | all-to-all | bytes 4194304 | tf_op jit(solution)/shard_map/all_to_all | solution.py:149
  185.9 1.3 copy-done.6
  187.2 1.2 fusion.27
  188.5 6.0 %fusion.6 = bf16[64,8,2048]{2,1,0:T(8,128)(2,1)} fusion(bf16[1,512,2048]{2,1,0:T(8,128)(2,1)S(1)} %copy-done, bf16[1,2048,512]{2,1,0:T(8,128)(2,1)} %param.22, bf16[64,8,2048]{2,1,0:T(8,128)(2,1)} %copy-done.6, f32[512,512]{1,0:T(8,128)S(1)} %fusion.27), kind=kOutput, calls=%fused_computation.20 | convolution fusion | flops 2150105088 | bytes 9437184 | tf_op jit(solution)/shard_map/dot_general | solution.py:154
  194.5 6.0 %all-to-all-start.2 = ((bf16[64,8,2048]{2,1,0:T(8,128)(2,1)}), bf16[64,8,2048]{2,1,0:T(8,128)(2,1)}, u32[]{:S(2)}, u32[]{:S(2)}) async-start(bf16[64,8,2048]{2,1,0:T(8,128)(2,1)} %fusion.6), calls=%async_computation.2 | async-start | bytes 4194304 | tf_op jit(solution)/shard_map/all_to_all | solution.py:157
  200.6 50.8 %all-to-all-done.2 = bf16[64,8,2048]{2,1,0:T(8,128)(2,1)} async-done(((bf16[64,8,2048]{2,1,0:T(8,128)(2,1)}), bf16[64,8,2048]{2,1,0:T(8,128)(2,1)}, u32[]{:S(2)}, u32[]{:S(2)}) %all-to-all-start.2) | async-done | bytes 2097184 | tf_op jit(solution)/shard_map/all_to_all | solution.py:157
  251.4 7.1 %gather_fusion.1 = bf16[512,2048]{1,0:T(8,128)(2,1)} fusion(bf16[512,2048]{1,0:T(8,128)(2,1)} %bitcast.32, s32[1024]{0:T(1024)S(1)} %pad_clamp_fusion), kind=kCustom, calls=%fused_computation.1 | custom fusion | bytes 4196352 | tf_op jit(solution)/shard_map/gather | solution.py:160
  258.5 5.4 %reshape.312 = f32[256,2,2048]{2,1,0:T(2,128)} reshape(bf16[512,2048]{1,0:T(8,128)(2,1)} %gather_fusion.1) | data formatting | bytes 6291456 | tf_op jit(solution)/shard_map/convert_element_type | solution.py:161
  263.9 9.0 %multiply_reduce_fusion = f32[256,2048]{1,0:T(8,128)S(1)} fusion(f32[256,2,2048]{2,1,0:T(2,128)} %reshape.312, f32[256,2]{1,0:T(8,128)S(1)} %copy.47), kind=kLoop, calls=%fused_computation.15 | loop fusion | flops 1572864 | bytes 6293504 | tf_op jit(solution)/shard_map/reduce_sum | solution.py:161
  272.9 1.3 fusion.19
  (77 shorter events, 1.4 us)
Async XLA Ops:
  6.5 182.0 %copy-start = (bf16[1,512,2048]{2,1,0:T(8,128)(2,1)S(1)}, bf16[1,512,2048]{2,1,0:T(8,128)(2,1)}, u32[]{:S(2)}) copy-start(bf16[1,512,2048]{2,1,0:T(8,128)(2,1)} %param.23) | copy-start | bytes 6291460
  6.5 0.8 copy-start.21
  6.5 17.1 %copy-start.20 = (s32[256,2]{0,1:T(2,128)S(1)}, s32[256,2]{0,1:T(2,128)}, u32[]{:S(2)}) copy-start(s32[256,2]{0,1:T(2,128)} %param.24) | copy-start | bytes 6148
  6.5 104.8 %all-gather.2.cloned.1.call-start = ((), (), s32[]{:S(2)}) async-start(), calls=%async_computation.3 | async-start | bytes 10485760 | tf_op jit(solution)/shard_map/all_gather | solution.py:118
  7.4 19.8 %copy-start.25 = (f32[8]{0:T(128)S(1)}, f32[8]{0:T(128)}, u32[]{:S(2)}) copy-start(f32[8]{0:T(128)} %param.17) | copy-start | bytes 100
  7.9 26.2 %collective-permute-start.1 = (bf16[128]{0:T(256)(128)(2,1)S(1)}, bf16[128]{0:T(256)(128)(2,1)S(1)}, u32[]{:S(2)}, u32[]{:S(2)}) collective-permute-start(bf16[128]{0:T(256)(128)(2,1)S(1)} %get-tuple-element.17), channel_id=1, source_target_pairs={{0,4},{4,8},{8,12},{12,16},{16,20},{20,24},{24,28},{28,32},{32,36}... | collective-permute-start | bytes 776 | tf_op jit(solution)/shard_map/ppermute | solution.py:19
  9.7 26.2 %collective-permute-start.4 = (bf16[128]{0:T(256)(128)(2,1)}, bf16[128]{0:T(256)(128)(2,1)}, u32[]{:S(2)}, u32[]{:S(2)}) collective-permute-start(bf16[128]{0:T(256)(128)(2,1)} %get-tuple-element.18), channel_id=1, source_target_pairs={{4,0},{8,4},{12,8},{16,12},{20,16},{24,20},{28,24},{32,28},{36,32}... | collective-permute-start | bytes 776 | tf_op jit(solution)/shard_map/ppermute | solution.py:22
  12.4 26.5 %collective-permute-start.2 = (bf16[128,128]{1,0:T(8,128)(2,1)}, bf16[128,128]{1,0:T(8,128)(2,1)S(1)}, u32[]{:S(2)}, u32[]{:S(2)}) collective-permute-start(bf16[128,128]{1,0:T(8,128)(2,1)} %get-tuple-element.9), channel_id=1, source_target_pairs={{0,4},{4,8},{8,12},{12,16},{16,20},{20,24},{24,28},{28,32},{32,36}... | collective-permute-start | bytes 98312 | tf_op jit(solution)/shard_map/ppermute | solution.py:19
  16.7 22.3 %collective-permute-start.5 = (bf16[128,128]{1,0:T(8,128)(2,1)}, bf16[128,128]{1,0:T(8,128)(2,1)S(1)}, u32[]{:S(2)}, u32[]{:S(2)}) collective-permute-start(bf16[128,128]{1,0:T(8,128)(2,1)} %get-tuple-element.10), channel_id=1, source_target_pairs={{4,0},{8,4},{12,8},{16,12},{20,16},{24,20},{28,24},{32,28},{36,32}... | collective-permute-start | bytes 98312 | tf_op jit(solution)/shard_map/ppermute | solution.py:22
  19.4 24.8 %collective-permute-start = (bf16[128,128]{1,0:T(8,128)(2,1)}, bf16[128,128]{1,0:T(8,128)(2,1)S(1)}, u32[]{:S(2)}, u32[]{:S(2)}) collective-permute-start(bf16[128,128]{1,0:T(8,128)(2,1)} %get-tuple-element.13), channel_id=1, source_target_pairs={{0,4},{4,8},{8,12},{12,16},{16,20},{20,24},{24,28},{28,32},{32,36}... | collective-permute-start | bytes 98312 | tf_op jit(solution)/shard_map/ppermute | solution.py:19
  29.0 7.6 %copy-start.9 = (s32[64,4,128]{2,0,1:T(8,128)}, s32[64,4,128]{2,0,1:T(8,128)S(1)}, u32[]{:S(2)}) copy-start(s32[64,4,128]{2,0,1:T(8,128)S(1)} %reduce-window.6) | copy-start | bytes 393220
  33.2 14.6 %copy-start.7 = (bf16[512,512]{0,1:T(8,128)(2,1)S(1)}, bf16[512,512]{0,1:T(8,128)(2,1)}, u32[]{:S(2)}) copy-start(bf16[512,512]{0,1:T(8,128)(2,1)} %copy.38) | copy-start | bytes 1572868
  33.2 17.6 %copy-start.15 = (s32[64,5]{0,1:T(8,128)}, s32[64,5]{0,1:T(8,128)S(1)}, u32[]{:S(2)}) copy-start(s32[64,5]{0,1:T(8,128)S(1)} %reduce-window.9) | copy-start | bytes 3844
  34.1 0.5 copy-start.23
  34.6 9.6 %collective-permute-start.3 = (bf16[128,128]{1,0:T(8,128)(2,1)}, bf16[128,128]{1,0:T(8,128)(2,1)S(1)}, u32[]{:S(2)}, u32[]{:S(2)}) collective-permute-start(bf16[128,128]{1,0:T(8,128)(2,1)} %get-tuple-element.14), channel_id=1, source_target_pairs={{4,0},{8,4},{12,8},{16,12},{20,16},{24,20},{28,24},{32,28},{36,32}... | collective-permute-start | bytes 98312 | tf_op jit(solution)/shard_map/ppermute | solution.py:22
  47.8 3.1 %copy-start.16 = (f32[2,4]{1,0:T(2,128)S(1)}, f32[2,4]{1,0:T(2,128)}, u32[]{:S(2)}) copy-start(f32[2,4]{1,0:T(2,128)} %max.32) | copy-start | bytes 100
  47.8 3.2 %copy-start.8 = (bf16[512,512]{0,1:T(8,128)(2,1)S(1)}, bf16[512,512]{0,1:T(8,128)(2,1)}, u32[]{:S(2)}) copy-start(bf16[512,512]{0,1:T(8,128)(2,1)} %copy.42) | copy-start | bytes 1572868
  47.8 3.2 %copy-start.13 = (bf16[768,128]{0,1:T(8,128)(2,1)S(1)}, bf16[768,128]{0,1:T(8,128)(2,1)}, u32[]{:S(2)}) copy-start(bf16[768,128]{0,1:T(8,128)(2,1)} %copy.41) | copy-start | bytes 589828
  57.6 3.2 %copy-start.14 = (bf16[768,128]{0,1:T(8,128)(2,1)S(1)}, bf16[768,128]{0,1:T(8,128)(2,1)}, u32[]{:S(2)}) copy-start(bf16[768,128]{0,1:T(8,128)(2,1)} %copy.36) | copy-start | bytes 589828
  60.8 5.9 %copy-start.12 = (bf16[768,128]{1,0:T(8,128)(2,1)S(1)}, bf16[768,128]{1,0:T(8,128)(2,1)}, u32[]{:S(2)}) copy-start(bf16[768,128]{1,0:T(8,128)(2,1)} %get-tuple-element.12) | copy-start | bytes 589828
  66.9 8.4 %copy-start.1 = (f32[2,768,512,4]{2,1,3,0:T(8,128)S(1)}, f32[2,768,512,4]{2,1,3,0:T(8,128)}, u32[]{:S(2)}) copy-start(f32[2,768,512,4]{2,1,3,0:T(8,128)} %get-tuple-element.26) | copy-start | bytes 37748740
  81.2 6.1 %slice-start = ((s32[64,5]{0,1:T(8,128)}), s32[64,4]{0,1:T(4,128)S(1)}, s32[]{:S(2)}) async-start(s32[64,5]{0,1:T(8,128)} %copy-done.15), calls=%async_computation.4 | async-start | bytes 4096 | tf_op jit(solution)/shard_map/slice.1
  81.2 6.1 %copy-start.18 = (s32[512]{0:T(512)S(1)}, s32[512]{0:T(512)}, u32[]{:S(2)}) copy-start(s32[512]{0:T(512)} %eq.65) | copy-start | bytes 6148
  81.2 6.2 %copy-start.19 = (s32[512,1]{0,1:T(1,128)S(1)}, s32[512,1]{0,1:T(1,128)}, u32[]{:S(2)}) copy-start(s32[512,1]{0,1:T(1,128)} %mul.81) | copy-start | bytes 6148
  82.3 5.0 %copy-start.10 = (s32[64,4,128]{2,0,1:T(8,128)S(1)}, s32[64,4,128]{2,0,1:T(8,128)}, u32[]{:S(2)}) copy-start(s32[64,4,128]{2,0,1:T(8,128)} %copy-done.9) | copy-start | bytes 393220
  82.3 26.6 %all-to-all-start = ((bf16[4,256,512]{2,1,0:T(8,128)(2,1)}), bf16[4,256,512]{2,1,0:T(8,128)(2,1)S(1)}, u32[]{:S(2)}, u32[]{:S(2)}) async-start(bf16[4,256,512]{2,1,0:T(8,128)(2,1)} %bitcast.120), calls=%async_computation | async-start | bytes 2097152 | tf_op jit(solution)/shard_map/all_to_all | solution.py:114
  108.9 1.0 copy-start.5
  111.3 5.3 %copy-start.4 = (bf16[2048,2048]{1,0:T(8,128)(2,1)S(1)}, bf16[2048,2048]{1,0:T(8,128)(2,1)}, u32[]{:S(2)}) copy-start(bf16[2048,2048]{1,0:T(8,128)(2,1)} %all-gather.2.cloned.1.call-done) | copy-start | bytes 25165828
  116.7 1.2 copy-start.11
  117.9 2.2 copy-start.17
  119.1 1.0 copy-start.2
  123.7 63.6 %copy-start.24 = (bf16[1,2048,512]{2,1,0:T(8,128)(2,1)S(1)}, bf16[1,2048,512]{2,1,0:T(8,128)(2,1)}, u32[]{:S(2)}) copy-start(bf16[1,2048,512]{2,1,0:T(8,128)(2,1)} %param.21) | copy-start | bytes 6291460
  185.9 1.3 copy-start.6
  194.5 6.0 %copy-start.22 = (f32[256,2]{0,1:T(2,128)S(1)}, f32[256,2]{0,1:T(2,128)}, u32[]{:S(2)}) copy-start(f32[256,2]{0,1:T(2,128)} %param.25) | copy-start | bytes 6148
  194.5 56.9 %all-to-all-start.2 = ((bf16[64,8,2048]{2,1,0:T(8,128)(2,1)}), bf16[64,8,2048]{2,1,0:T(8,128)(2,1)}, u32[]{:S(2)}, u32[]{:S(2)}) async-start(bf16[64,8,2048]{2,1,0:T(8,128)(2,1)} %fusion.6), calls=%async_computation.2 | async-start | bytes 4194304 | tf_op jit(solution)/shard_map/all_to_all | solution.py:157
  263.9 9.0 %copy-start.3 = (bf16[256,2048]{1,0:T(8,128)(2,1)S(1)}, bf16[256,2048]{1,0:T(8,128)(2,1)}, u32[]{:S(2)}) copy-start(bf16[256,2048]{1,0:T(8,128)(2,1)} %copy-done.2) | copy-start | bytes 3145732
Sparse Core Ops, SparseCore 0:
  9.1 94.3 all-gather.1
where the time goes:
time: 282 us; the launch traced here: 281 us
  waiting for transfers between devices  70.5 us (25%)
  blocking collectives  62.2 us (22%)
  local copies, waits for them, and re-layouts  43.8 us (16%)
  matrix products  33.4 us (12%)
  other arithmetic  32.1 us (11%)
  starting transfers between devices  25.1 us (9%)
  between operations  13.8 us (5%)
    all_to_all x1, blocking collectives, per_device(): lax.all_to_all(outgoing, 'sp', split_axis=0, concat_axis=0, tiled=True)  62.2 us
    all_to_all x1, waiting for transfers between devices, per_device(): lax.all_to_all(produced.reshape(incoming.shape), 'sp', split_axis=0, conc...  50.8 us
    all_to_all x1, waiting for transfers between devices, per_device(): lax.all_to_all(attended, 'tp', split_axis=0, concat_axis=1, tiled=True)  18.9 us
    ppermute x3, starting transfers between devices, extended(): lax.ppermute(lax.slice_in_dim(block, block.shape[dim] - width, None, axis...  10.3 us
    reduce_sum x2, other arithmetic, attend(): jnp.sum(exponent, axis=3, keepdims=True) + jnp.exp(sink_col - row_top)  10 us
    dot_general x2, matrix products, attend(): jnp.einsum('qgrd,kgd->grqk', query_heads, key_heads, preferred_element_ty...  9.67 us
    dot_general x2, matrix products, attend(): jnp.einsum('grqk,kgd->qgrd', attn_weight, value_heads, preferred_element_...  9.31 us
    reduce_sum x1, other arithmetic, per_device(): jnp.sum(route_weights[:, :, None] * route_out.astype(jnp.float32), axis=1)  8.96 us
  transfers between devices with their start and end apart: 9, of which 2 were waited for; matrix products, arithmetic and copies ran while one was open for 22% of the time, Pallas kernels for 0%

commit v1 on v0

v1 whole, which is shorter than its diff:
```python
import jax
import jax.numpy as jnp
from jax import lax
from jax.experimental import pallas as pl
from jax.experimental.pallas import tpu as pltpu
from jax.sharding import PartitionSpec as P

HD = 64
WINDOW = 128
NEG = -1e30
EPS = 1e-06
F32 = jnp.float32
BF16 = jnp.bfloat16
NT = (((1,), (1,)), ((), ()))
TN = (((0,), (0,)), ((), ()))
VMEM = pl.BlockSpec(memory_space=pltpu.VMEM)


def pack_body(k_ref, v_ref, doc_ref, low_ref, high_ref):
    rows = k_ref.shape[0]
    docs = (doc_ref[...] + 1).astype(F32)
    last = docs.shape[0] - 1
    for ref, start, row in ((low_ref, 0, 0), (high_ref, rows - WINDOW, last)):
        ref[0:WINDOW, 0:128] = k_ref[start : start + WINDOW, :]
        ref[0:WINDOW, 128:256] = v_ref[start : start + WINDOW, :]
        line = jnp.broadcast_to(docs[row : row + 1, :], (16, 128)).astype(BF16)
        ref[WINDOW : WINDOW + 16, 0:128] = line
        ref[WINDOW : WINDOW + 16, 128:256] = line


def slots_body(routes_ref, slots_ref, *, experts, capacity):
    rows = routes_ref.shape[1]
    first = routes_ref[0:1, :]
    second = routes_ref[1:2, :]
    ids = lax.broadcasted_iota(jnp.int32, (experts, rows), 0)
    named = jnp.where((ids == first) | (ids == second), 1.0, 0.0)
    before = lax.broadcasted_iota(jnp.int32, (rows, rows), 0) < lax.broadcasted_iota(
        jnp.int32, (rows, rows), 1
    )
    earlier = jnp.dot(
        named.astype(BF16),
        jnp.where(before, 1.0, 0.0).astype(BF16),
        preferred_element_type=F32,
    )
    for k, route in ((0, first), (1, second)):
        rank = jnp.sum(jnp.where(ids == route, earlier, 0.0), axis=0, keepdims=True)
        slots_ref[k : k + 1, :] = route * capacity + rank.astype(jnp.int32)


def attend_body(q_ref, k_ref, v_ref, doc_ref, low_ref, high_ref, sink_ref, out_ref, kvar, vt, kdoc):
    block = pl.program_id(0)
    rows = k_ref.shape[0]

    @pl.when(block == 0)
    def _():
        lane = lax.broadcasted_iota(jnp.int32, (WINDOW, 128), 1)
        count = rows // WINDOW + 2
        for part in range(count):
            here = slice(part * WINDOW, (part + 1) * WINDOW)
            if part == 0:
                keys = low_ref[0:WINDOW, 0:128]
                values = low_ref[0:WINDOW, 128:256]
                docs = low_ref[WINDOW : WINDOW + 1, 0:128].astype(F32)
            elif part == count - 1:
                keys = high_ref[0:WINDOW, 0:128]
                values = high_ref[0:WINDOW, 128:256]
                docs = high_ref[WINDOW : WINDOW + 1, 0:128].astype(F32)
            else:
                keys = k_ref[(part - 1) * WINDOW : part * WINDOW, :]
                values = v_ref[(part - 1) * WINDOW : part * WINDOW, :]
                docs = (doc_ref[part - 1 : part, :] + 1).astype(F32)
            scaled = keys.astype(F32) * HD ** (-0.5)
            turned = pltpu.roll(scaled, 64, 1)
            left = lane < 64
            kvar[0, here, :] = jnp.where(left, scaled, 0.0).astype(BF16)
            kvar[1, here, :] = jnp.where(left, 0.0, turned).astype(BF16)
            kvar[2, here, :] = jnp.where(left, turned, 0.0).astype(BF16)
            kvar[3, here, :] = jnp.where(left, 0.0, scaled).astype(BF16)
            vt[:, here] = values.T
            kdoc[here, :] = jnp.broadcast_to(docs, (WINDOW, 128)).T

    start = pl.multiple_of(block * WINDOW, WINDOW)
    span = 3 * WINDOW
    query_docs = (doc_ref[pl.ds(block, 1), :] + 1).astype(F32)
    ahead = lax.broadcasted_iota(jnp.int32, (span, WINDOW), 0) - lax.broadcasted_iota(
        jnp.int32, (span, WINDOW), 1
    )
    allowed = (ahead >= 0) & (ahead <= 2 * WINDOW) & (kdoc[pl.ds(start, span), :] == query_docs)
    bias = jnp.where(allowed, 0.0, NEG)
    groups = k_ref.shape[1] // HD
    ratio = q_ref.shape[1] // k_ref.shape[1]
    for pair in range(groups * ratio // 2):
        group = pair // (ratio // 2)
        queries = q_ref[:, pair * 128 : (pair + 1) * 128]
        halves = []
        for half in range(2):
            head = pair * 2 + half
            scores = lax.dot_general(
                kvar[group * 2 + half, pl.ds(start, span), :],
                queries,
                NT,
                preferred_element_type=F32,
            )
            scores = scores + bias
            sink = sink_ref[head]
            top = jnp.maximum(jnp.max(scores, axis=0, keepdims=True), sink)
            weight = jnp.exp(scores - top)
            total = jnp.sum(weight, axis=0, keepdims=True) + jnp.exp(sink - top)
            halves.append((weight * (1.0 / total)).astype(BF16))
        both = jnp.concatenate(halves, axis=1)
        mixed = jnp.dot(
            vt[group * HD : (group + 1) * HD, pl.ds(start, span)],
            both,
            preferred_element_type=F32,
        )
        stacked = jnp.concatenate([mixed[:, 0:128], mixed[:, 128:256]], axis=0)
        out_ref[:, pair * 128 : (pair + 1) * 128] = stacked.T.astype(BF16)


def project_body(
    core_ref,
    here_att,
    there_att,
    here_w,
    there_w,
    residual_ref,
    gain_ref,
    slots_ref,
    out_ref,
    stream_ref,
    acc,
):
    step = pl.program_id(0)
    partial = jnp.dot(here_att[0], here_w[0], preferred_element_type=F32) + jnp.dot(
        there_att[0], there_w[0], preferred_element_type=F32
    )
    partial = partial.astype(BF16).astype(F32)

    @pl.when(step == 0)
    def _():
        acc[...] = partial

    @pl.when(step > 0)
    def _():
        acc[...] += partial

    @pl.when(step == pl.num_programs(0) - 1)
    def _():
        stream = (residual_ref[...].astype(F32) + acc[...]).astype(BF16)
        stream_ref[...] = stream
        wide = stream.astype(F32)
        scale = lax.rsqrt(jnp.mean(wide * wide, axis=1, keepdims=True) + EPS)
        normed = (wide * scale * gain_ref[...]).astype(BF16)
        ids = lax.broadcasted_iota(jnp.int32, (out_ref.shape[0], slots_ref.shape[1]), 0)
        place = (ids == slots_ref[0:1, :]) | (ids == slots_ref[1:2, :])
        out_ref[...] = jnp.dot(
            jnp.where(place, 1.0, 0.0).astype(BF16), normed, preferred_element_type=F32
        ).astype(BF16)


def expert_body(x_ref, gate_ref, up_ref, down_ref, out_ref, acc):
    step = pl.program_id(0)
    gate_act = jnp.dot(x_ref[...], gate_ref[0], preferred_element_type=F32)
    up_act = jnp.dot(x_ref[...], up_ref[0], preferred_element_type=F32)
    hidden = (gate_act / (1.0 + jnp.exp(-gate_act)) * up_act).astype(BF16)
    part = jnp.dot(hidden, down_ref[0], preferred_element_type=F32)
    last = pl.num_programs(0) - 1

    @pl.when(step == 0)
    def _():
        acc[...] = part

    @pl.when((step > 0) & (step < last))
    def _():
        acc[...] += part

    @pl.when(step == last)
    def _():
        out_ref[...] = (acc[...] + part).astype(BF16)


def combine_body(back_ref, stream_ref, slots_ref, weights_ref, out_ref):
    rows = stream_ref.shape[0]
    slots = back_ref.shape[0]
    width = stream_ref.shape[1]
    ids = lax.broadcasted_iota(jnp.int32, (slots, rows), 0)
    total = None
    for k in range(2):
        pick = jnp.where(ids == slots_ref[k : k + 1, :], 1.0, 0.0).astype(BF16)
        chosen = lax.dot_general(pick, back_ref[...], TN, preferred_element_type=F32)
        line = weights_ref[k : k + 1, :]
        columns = [
            jnp.broadcast_to(line[:, i : i + 128], (128, 128)).T for i in range(0, rows, 128)
        ]
        factor = jnp.concatenate(columns, axis=0)
        factor = jnp.concatenate([factor] * (width // 128), axis=1)
        term = factor * chosen
        total = term if total is None else total + term
    out_ref[...] = (stream_ref[...].astype(F32) + total).astype(BF16)


def per_device(
    queries,
    key_rows,
    value_rows,
    doc_ids,
    sink_logit,
    residual,
    out_weight,
    norm_gain,
    gate_weight,
    up_weight,
    down_weight,
    routes,
    route_weights,
):
    local_rows = queries.shape[0]
    home_rows, width = residual.shape
    devices = lax.axis_size("sp")
    ways = lax.axis_size("tp")
    experts = devices * gate_weight.shape[0]
    route_count = routes.shape[1]
    capacity = route_count * home_rows // experts
    slot_count = experts * capacity
    shard = out_weight.shape[0]
    core = lax.axis_index("sp") % 2
    half_weight = lax.dynamic_slice_in_dim(out_weight, core * (shard // 2), shard // 2, 0)
    here_weight = lax.all_gather(half_weight, "tp", axis=0)

    doc_lines = doc_ids.reshape(local_rows // 128, 128)
    halo = jax.ShapeDtypeStruct((WINDOW + 16, 256), BF16)
    first_rows, last_rows = pl.pallas_call(
        pack_body,
        out_shape=(halo, halo),
        in_specs=[VMEM] * 3,
        out_specs=(VMEM, VMEM),
        name="pack",
    )(key_rows, value_rows, doc_lines)
    forward = [(i, i + 1) for i in range(devices - 1)]
    backward = [(j, i) for i, j in forward]
    low = lax.ppermute(last_rows, "sp", forward)
    high = lax.ppermute(first_rows, "sp", backward)

    slots = pl.pallas_call(
        lambda r, s: slots_body(r, s, experts=experts, capacity=capacity),
        out_shape=jax.ShapeDtypeStruct((route_count, home_rows), jnp.int32),
        in_specs=[VMEM],
        out_specs=VMEM,
        name="slots",
    )(routes.T)

    blocks = local_rows // WINDOW
    whole = lambda shape: pl.BlockSpec(shape, lambda i: (0,) * len(shape))
    attended = pl.pallas_call(
        attend_body,
        grid=(blocks,),
        out_shape=jax.ShapeDtypeStruct(queries.shape, BF16),
        in_specs=[
            pl.BlockSpec((WINDOW, queries.shape[1]), lambda i: (i, 0)),
            whole(key_rows.shape),
            whole(value_rows.shape),
            whole(doc_lines.shape),
            whole(halo.shape),
            whole(halo.shape),
            pl.BlockSpec(memory_space=pltpu.SMEM),
        ],
        out_specs=pl.BlockSpec((WINDOW, queries.shape[1]), lambda i: (i, 0)),
        scratch_shapes=[
            pltpu.VMEM((4, local_rows + 2 * WINDOW, 128), BF16),
            pltpu.VMEM((128, local_rows + 2 * WINDOW), BF16),
            pltpu.VMEM((local_rows + 2 * WINDOW, 128), F32),
        ],
        name="attend",
    )(queries, key_rows, value_rows, doc_lines, low, high, sink_logit)

    columns = queries.shape[1]
    regrouped = lax.all_to_all(
        attended.reshape(ways, home_rows, columns), "tp", split_axis=0, concat_axis=0, tiled=True
    )
    swap = [(i, i ^ 1) for i in range(devices)]
    there_weight = lax.ppermute(here_weight, "sp", swap)

    fixed = lambda shape: pl.BlockSpec(shape, lambda i, c: (0,) * len(shape))
    outgoing, stream = pl.pallas_call(
        project_body,
        grid_spec=pltpu.PrefetchScalarGridSpec(
            num_scalar_prefetch=1,
            grid=(ways,),
            in_specs=[
                pl.BlockSpec((1, home_rows, columns // 2), lambda i, c: (i, 0, c[0])),
                pl.BlockSpec((1, home_rows, columns // 2), lambda i, c: (i, 0, 1 - c[0])),
                pl.BlockSpec((1, shard // 2, width), lambda i, c: (i, 0, 0)),
                pl.BlockSpec((1, shard // 2, width), lambda i, c: (i, 0, 0)),
                fixed((home_rows, width)),
                fixed((1, width)),
                fixed((route_count, home_rows)),
            ],
            out_specs=[fixed((slot_count, width)), fixed((home_rows, width))],
            scratch_shapes=[pltpu.VMEM((home_rows, width), F32)],
        ),
        out_shape=(
            jax.ShapeDtypeStruct((slot_count, width), BF16),
            jax.ShapeDtypeStruct((home_rows, width), BF16),
        ),
        name="project",
    )(
        core.astype(jnp.int32).reshape(1),
        regrouped,
        regrouped,
        here_weight,
        there_weight,
        residual,
        norm_gain.reshape(1, width),
        slots,
    )

    incoming = lax.all_to_all(
        outgoing.reshape(devices, -1, width), "sp", split_axis=0, concat_axis=0, tiled=True
    )
    hidden_units = gate_weight.shape[2]
    pieces = 2
    piece = hidden_units // pieces
    produced = pl.pallas_call(
        expert_body,
        grid=(pieces,),
        out_shape=jax.ShapeDtypeStruct((slot_count, width), BF16),
        in_specs=[
            whole((slot_count, width)),
            pl.BlockSpec((1, width, piece), lambda i: (0, 0, i)),
            pl.BlockSpec((1, width, piece), lambda i: (0, 0, i)),
            pl.BlockSpec((1, piece, width), lambda i: (0, i, 0)),
        ],
        out_specs=whole((slot_count, width)),
        scratch_shapes=[pltpu.VMEM((slot_count, width), F32)],
        name="experts",
    )(incoming.reshape(slot_count, width), gate_weight, up_weight, down_weight)
    returned = lax.all_to_all(
        produced.reshape(devices, -1, width), "sp", split_axis=0, concat_axis=0, tiled=True
    )
    half = width // 2
    return pl.pallas_call(
        combine_body,
        grid=(2,),
        out_shape=jax.ShapeDtypeStruct((home_rows, width), BF16),
        in_specs=[
            pl.BlockSpec((slot_count, half), lambda i: (0, i)),
            pl.BlockSpec((home_rows, half), lambda i: (0, i)),
            whole((route_count, home_rows)),
            whole((route_count, home_rows)),
        ],
        out_specs=pl.BlockSpec((home_rows, half), lambda i: (0, i)),
        name="combine",
    )(returned.reshape(slot_count, width), stream, slots, route_weights.T)


def solution(mesh):
    return jax.shard_map(
        per_device,
        mesh=mesh,
        in_specs=(
            P("sp", "tp"),
            P("sp", "tp"),
            P("sp", "tp"),
            P("sp"),
            P("tp"),
            P(("sp", "tp"), None),
            P("tp", None),
            P(),
            P("sp", None, None),
            P("sp", None, None),
            P("sp", None, None),
            P(("sp", "tp"), None),
            P(("sp", "tp"), None),
        ),
        out_specs=P(("sp", "tp"), None),
        check_vma=False,
    )
```

time: 282 us -> 257 us (0.911)
  blocking collectives: 62.2 us -> 122 us
  Pallas kernels: 0 us -> 40.3 us
  local copies, waits for them, and re-layouts: 43.8 us -> 4.26 us
  matrix products: 33.4 us -> 0 us
  other arithmetic: 32.1 us -> 0 us
  starting transfers between devices: 25.1 us -> 8.37 us
  waiting for transfers between devices: 70.5 us -> 67.4 us
    all_to_all x1 -> x2, blocking collectives: 62.2 us -> 122 us  [the longest x1 65.1 us: per_device(): lax.all_to_all(outgoing.reshape(devices, -1, width), 'sp', split_axis=0,...]
    all_to_all x2 -> x1, waiting for transfers between devices: 69.7 us -> 11.6 us  [per_device(): lax.all_to_all(attended.reshape(ways, home_rows, columns), 'tp', split_ax...]
    all_gather x1, waiting for transfers between devices: 0.02 us -> 53.2 us  [per_device(): here_weight = lax.all_gather(half_weight, 'tp', axis=0)]
    pallas_call x0 -> x6, Pallas kernels: none -> 40.3 us  [the longest x1 15.5 us: per_device(): pl.pallas_call(attend_body, grid=(blocks,), out_shape=jax.ShapeDtypeStruc...]
    dot_general x10 -> x0, matrix products: 33.4 us -> none  [the longest x2 9.67 us: attend(): jnp.einsum('qgrd,kgd->grqk', query_heads, key_heads, preferred_element_ty...]
    reduce_sum x4 -> x0, other arithmetic: 19.1 us -> none  [the longest x2 10 us: attend(): jnp.sum(exponent, axis=3, keepdims=True) + jnp.exp(sink_col - row_top)]
    slice x12 -> x0, local copies, waits for them, and re-layouts: 13 us -> none  [the longest x2 3.5 us: per_device(): padded_keys[row_start:key_end]]
    ppermute x6 -> x3, starting transfers between devices: 14.1 us -> 3.7 us  [the longest x1 2.4 us: per_device(): low = lax.ppermute(last_rows, 'sp', forward)]
  transfers between devices with their start and end apart: 9 -> 5, of which waited for: 2 -> 4; matrix products, arithmetic and copies ran while one was open for 22% -> 0% of each run, Pallas kernels for 0% -> 7%
where the time goes in v1:
time: 257 us; the launch traced here: 256 us
  blocking collectives  122 us (47%)
  waiting for transfers between devices  67.4 us (26%)
  Pallas kernels  40.3 us (16%)
  between operations  13.4 us (5%)
  starting transfers between devices  8.37 us (3%)
  local copies, waits for them, and re-layouts  4.26 us (2%)
    all_to_all x1, blocking collectives, per_device(): lax.all_to_all(outgoing.reshape(devices, -1, width), 'sp', split_axis=0,...  65.1 us
    all_to_all x1, blocking collectives, per_device(): lax.all_to_all(produced.reshape(devices, -1, width), 'sp', split_axis=0,...  56.8 us
    all_gather x1, waiting for transfers between devices, per_device(): here_weight = lax.all_gather(half_weight, 'tp', axis=0)  53.2 us
    pallas_call x1, Pallas kernels, per_device(): pl.pallas_call(attend_body, grid=(blocks,), out_shape=jax.ShapeDtypeStruc...  15.5 us
    all_to_all x1, waiting for transfers between devices, per_device(): lax.all_to_all(attended.reshape(ways, home_rows, columns), 'tp', split_ax...  11.6 us
    pallas_call x1, Pallas kernels, per_device(): pl.pallas_call(project_body, grid_spec=pltpu.PrefetchScalarGridSpec(num_s...  9.42 us
    pallas_call x1, Pallas kernels, per_device(): pl.pallas_call(expert_body, grid=(pieces,), out_shape=jax.ShapeDtypeStruc...  8.44 us
  transfers between devices with their start and end apart: 5, of which 4 were waited for; matrix products, arithmetic and copies ran while one was open for 0% of the time, Pallas kernels for 7%

profile of v1, /device:TPU:8, one launch (start us, length us, event | category | flops | bytes accessed | tf_op | source)
XLA Modules:
  0.0 255.7 jit_solution(6286828047162259928)
XLA Ops:
  6.5 0.0 copy-start
  6.5 0.0 all-gather.3.cloned.1.call-start
  6.5 1.6 copy-done
  8.1 1.1 constant_dynamic-slice_fusion
  9.2 0.0 all-gather.3.cloned.1.call-update
  9.2 53.2 %all-gather.3.cloned.1.call-done = bf16[1024,2048]{1,0:T(8,128)(2,1)} async-done(((bf16[256,2048]{1,0:T(8,128)(2,1)}), bf16[1024,2048]{1,0:T(8,128)(2,1)}) %all-gather.3.cloned.1.call-update) | async-done | bytes 4194320 | tf_op jit(solution)/shard_map/all_gather | solution.py:228
  62.4 0.0 collective-permute-start.2
  62.4 1.7 pack.1
  64.1 2.4 collective-permute-start
  66.5 1.3 collective-permute-start.1
  67.8 1.7 collective-permute-done.low_ref
  69.5 0.0 copy-start.2
  69.5 0.9 collective-permute-done.1.high_ref
  70.5 0.0 copy-done.2
  70.5 0.0 copy-start.3
  70.5 0.6 copy-done.3
  71.1 15.5 %attend.1 = bf16[1024,512]{1,0:T(8,128)(2,1)} custom-call(bf16[1024,512]{1,0:T(8,128)(2,1)} %q_ref.1, bf16[1024,128]{1,0:T(8,128)(2,1)} %k_ref.3, bf16[1024,128]{1,0:T(8,128)(2,1)} %v_ref.3, s32[8,128]{1,0:T(8,128)} %bitcast.19, bf16[144,256]{1,0:T(8,128)(2,1)} %copy-done.2, bf16[144,256]{1,0:T(8,128)(2,1)} %copy-done.3, f32[8]{0:T(128)} %sink_ref.1), custom_call_target="tpu_custom_call" | custom-call | tf_op jit(solution)/shard_map/attend/pallas_call | solution.py:254
  86.6 4.7 %all-to-all-start = ((bf16[4,256,512]{2,1,0:T(8,128)(2,1)}), bf16[4,256,512]{2,1,0:T(8,128)(2,1)S(1)}, u32[]{:S(2)}, u32[]{:S(2)}) async-start(bf16[4,256,512]{2,1,0:T(8,128)(2,1)} %bitcast.16), calls=%async_computation | async-start | bytes 2097152 | tf_op jit(solution)/shard_map/all_to_all | solution.py:277
  91.3 1.4 slots.1.slots_ref
  92.7 11.6 %all-to-all-done.here_att.there_att = bf16[4,256,512]{2,1,0:T(8,128)(2,1)S(1)} async-done(((bf16[4,256,512]{2,1,0:T(8,128)(2,1)}), bf16[4,256,512]{2,1,0:T(8,128)(2,1)S(1)}, u32[]{:S(2)}, u32[]{:S(2)}) %all-to-all-start) | async-done | bytes 1048608 | tf_op jit(solution)/shard_map/all_to_all | solution.py:277
  104.3 0.0 copy-start.1
  104.3 0.0 collective-permute-done.2.there_w
  104.3 1.0 copy-done.1
  105.3 9.4 %project.1 = (bf16[512,2048]{1,0:T(8,128)(2,1)}, bf16[256,2048]{1,0:T(8,128)(2,1)}) custom-call(s32[1]{0:T(128)} %bitcast.core_ref, bf16[4,256,512]{2,1,0:T(8,128)(2,1)} %copy-done.1, bf16[4,256,512]{2,1,0:T(8,128)(2,1)} %copy-done.1, bf16[4,256,2048]{2,1,0:T(8,128)(2,1)} %bitcast.15, bf16[4,256,2048]{2,1,0:T(8,128)(2,1)} %collective-permute-done.2.there_w, ...), custom_call_target="tpu_custom_call" | custom-call | tf_op jit(solution)/shard_map/project/pallas_call | solution.py:284
  114.7 65.1 %all_to_all.15 = bf16[64,8,2048]{2,1,0:T(8,128)(2,1)} all-to-all(bf16[64,8,2048]{2,1,0:T(8,128)(2,1)} %bitcast.17), channel_id=1, replica_groups=mesh['sp'=64,'tp'=4] {'sp'}, dimensions={0} | all-to-all | bytes 4194304 | tf_op jit(solution)/shard_map/all_to_all | solution.py:317
  179.8 8.4 %experts.1 = bf16[512,2048]{1,0:T(8,128)(2,1)} custom-call(bf16[512,2048]{1,0:T(8,128)(2,1)} %bitcast.11, bf16[1,2048,512]{2,1,0:T(8,128)(2,1)} %gate_ref.1, bf16[1,2048,512]{2,1,0:T(8,128)(2,1)} %up_ref.1, bf16[1,512,2048]{2,1,0:T(8,128)(2,1)} %down_ref.1), custom_call_target="tpu_custom_call" | custom-call | tf_op jit(solution)/shard_map/experts/pallas_call | solution.py:323
  188.3 56.8 %all_to_all.16 = bf16[64,8,2048]{2,1,0:T(8,128)(2,1)} all-to-all(bf16[64,8,2048]{2,1,0:T(8,128)(2,1)} %bitcast.12), channel_id=1, replica_groups=mesh['sp'=64,'tp'=4] {'sp'}, dimensions={0} | all-to-all | bytes 4194304 | tf_op jit(solution)/shard_map/all_to_all | solution.py:337
  245.1 3.8 %combine.1 = bf16[256,2048]{1,0:T(8,128)(2,1)} custom-call(bf16[512,2048]{1,0:T(8,128)(2,1)} %bitcast.13, bf16[256,2048]{1,0:T(8,128)(2,1)} %get-tuple-element.12.stream_ref, s32[2,256]{1,0:T(2,128)} %slots.1.slots_ref, f32[2,256]{1,0:T(2,128)} %bitcast.21), custom_call_target="tpu_custom_call" | custom-call | tf_op jit(solution)/shard_map/combine/pallas_call | solution.py:341
Async XLA Ops:
  6.5 1.6 copy-start
  6.5 55.9 %all-gather.3.cloned.1.call-start = ((), (), s32[]{:S(2)}) async-start(), calls=%async_computation.3 | async-start | bytes 5242880 | tf_op jit(solution)/shard_map/all_gather | solution.py:228
  62.4 41.9 %collective-permute-start.2 = (bf16[4,256,2048]{2,1,0:T(8,128)(2,1)}, bf16[4,256,2048]{2,1,0:T(8,128)(2,1)}, u32[]{:S(2)}, u32[]{:S(2)}) collective-permute-start(bf16[4,256,2048]{2,1,0:T(8,128)(2,1)} %bitcast.14), channel_id=1, source_target_pairs={{0,4},{4,0},{8,12},{12,8},{16,20},{20,16},{24,28},{28,24},{32,36},... | collective-permute-start | bytes 12582920 | tf_op jit(solution)/shard_map/ppermute | solution.py:281
  64.1 5.4 %collective-permute-start = (bf16[144,256]{1,0:T(8,128)(2,1)}, bf16[144,256]{1,0:T(8,128)(2,1)S(1)}, u32[]{:S(2)}, u32[]{:S(2)}) collective-permute-start(bf16[144,256]{1,0:T(8,128)(2,1)} %get-tuple-element.9), channel_id=1, source_target_pairs={{0,4},{4,8},{8,12},{12,16},{16,20},{20,24},{24,28},{28,32},{32,36}... | collective-permute-start | bytes 221192 | tf_op jit(solution)/shard_map/ppermute | solution.py:241
  66.5 3.9 %collective-permute-start.1 = (bf16[144,256]{1,0:T(8,128)(2,1)}, bf16[144,256]{1,0:T(8,128)(2,1)S(1)}, u32[]{:S(2)}, u32[]{:S(2)}) collective-permute-start(bf16[144,256]{1,0:T(8,128)(2,1)} %get-tuple-element.10), channel_id=1, source_target_pairs={{4,0},{8,4},{12,8},{16,12},{20,16},{24,20},{28,24},{32,28},{36,32}... | collective-permute-start | bytes 221192 | tf_op jit(solution)/shard_map/ppermute | solution.py:242
  69.5 0.9 copy-start.2
  70.5 0.6 copy-start.3
  86.6 17.7 %all-to-all-start = ((bf16[4,256,512]{2,1,0:T(8,128)(2,1)}), bf16[4,256,512]{2,1,0:T(8,128)(2,1)S(1)}, u32[]{:S(2)}, u32[]{:S(2)}) async-start(bf16[4,256,512]{2,1,0:T(8,128)(2,1)} %bitcast.16), calls=%async_computation | async-start | bytes 2097152 | tf_op jit(solution)/shard_map/all_to_all | solution.py:277
  104.3 1.0 copy-start.1
Sparse Core Ops, SparseCore 0:
  9.4 52.9 all-gather.2
